TPU v7x, 32 devices: a whole 2x2x4 slice. The times are simulated.
32 devices in a mesh: ep: 16 (over z, y, x), tp: 2 (over core).
Axes of the slice: x: 2, y: 2, z: 4, core: 2. Of those that a mesh axis runs over, the one named last changes fastest.
Arguments:
- tokens: bfloat16 [256, 2048], P('ep'), may hold values from -6 to 6
- cache_keys: bfloat16 [256, 2, 64, 1024], P('ep', 'tp'), may hold values from -6 to 6
- cache_values: bfloat16 [256, 2, 64, 1024], P('ep', 'tp'), may hold values from -6 to 6
- cache_lengths: int32 [256], P('ep'), may hold values from 1 to 1024, as said below
- norm_in: float32 [2048], replicated, may hold values from 0.1 to 1.9
- w_query: bfloat16 [2048, 512], P(None, 'tp'), may hold values from -0.125 to 0.125
- w_key: bfloat16 [2048, 128], P(None, 'tp'), may hold values from -0.125 to 0.125
- w_value: bfloat16 [2048, 128], P(None, 'tp'), may hold values from -0.125 to 0.125
- stick_bias: float32 [8], P('tp'), may hold values from -8 to -1.5
- w_output: bfloat16 [512, 2048], P('tp'), may hold values from -0.75 to 0.75
- norm_mid: float32 [2048], replicated, may hold values from 0.1 to 1.9
- routes: int32 [256, 6], P('ep'), may hold values from 0 to 15, all different within a row; in each aligned block of 16 rows (0 to 15, 16 to 31, ...) at most 6 rows name the same one
- route_weights: float32 [256, 6], P('ep'), may hold values from 0.1 to 1
- expert_gate: bfloat16 [16, 2048, 512], P('ep', None, 'tp'), may hold values from -0.125 to 0.125
- expert_up: bfloat16 [16, 2048, 512], P('ep', None, 'tp'), may hold values from -0.125 to 0.125
- expert_down: bfloat16 [16, 512, 2048], P('ep', 'tp'), may hold values from -0.25 to 0.25
- dense_gate: bfloat16 [2048, 256], P('ep'), may hold values from -0.125 to 0.125
- dense_up: bfloat16 [2048, 256], P('ep'), may hold values from -0.125 to 0.125
- dense_down: bfloat16 [256, 2048], P(None, 'ep'), may hold values from -0.375 to 0.375
- mix_gate: float32 [2048], replicated, may hold values from -0.125 to 0.125
- norm_out: float32 [2048], replicated, may hold values from 0.1 to 1.9
Outputs:
- mixed: bfloat16 [256, 2048], P('ep')
- fresh_keys: bfloat16 [256, 128], P('ep', 'tp')
- fresh_values: bfloat16 [256, 128], P('ep', 'tp')
Inputs may be any that keep to these rules, and one draw needn't show every extreme that they name: `cache_lengths`: positions at or past a sequence's length are not read. Among the sequences of one index of ep some sequence has length 1024. `routes`: each row names 6 different experts; among the rows of one index of ep (aligned blocks of 16 rows) no expert is named by more than 6 rows, and that bound is reached.
All inputs are finite; a program needn't handle non-finite values.
Results may differ from a plain program's by a relative error of at most 0.015.
Values may be sent and summed in bfloat16 or wider, within the bound.
A program may use at most 64 MiB of HBM per device.

v0:
```python
import jax
import jax.numpy as jnp
from jax import lax
from jax.sharding import PartitionSpec as P


def layer_norm(values, gain):
    floats = values.astype(jnp.float32)
    center = jnp.mean(floats, -1, keepdims=True)
    spread = jnp.mean(jnp.square(floats - center), -1, keepdims=True)
    return (floats - center) * lax.rsqrt(spread + 1e-05) * gain


def later_positions(log_keep):
    length = log_keep.shape[-1]
    span = 128
    count = length // span
    lead = log_keep.shape[:-1]
    blocks = log_keep.reshape(lead + (count, span))
    inner = jnp.arange(span)
    within_table = (inner[:, None] > inner[None, :]).astype(jnp.float32)
    within = jnp.einsum("...nb,bc->...nc", blocks, within_table, precision=lax.Precision.HIGHEST)
    totals = jnp.sum(blocks, axis=-1)
    outer = jnp.arange(count)
    outer_table = (outer[:, None] > outer[None, :]).astype(jnp.float32)
    carried = jnp.einsum("...m,mn->...n", totals, outer_table, precision=lax.Precision.HIGHEST)
    return (within + carried[..., None]).reshape(lead + (length,))


def shards(
    tokens,
    cache_keys,
    cache_values,
    cache_lengths,
    norm_in,
    w_query,
    w_key,
    w_value,
    stick_bias,
    w_output,
    norm_mid,
    routes,
    route_weights,
    expert_gate,
    expert_up,
    expert_down,
    dense_gate,
    dense_up,
    dense_down,
    mix_gate,
    norm_out,
):
    normed = layer_norm(tokens, norm_in).astype(jnp.bfloat16)
    queries = jnp.dot(normed, w_query, preferred_element_type=jnp.float32).astype(jnp.bfloat16)
    fresh_keys = jnp.dot(normed, w_key, preferred_element_type=jnp.float32).astype(jnp.bfloat16)
    fresh_values = jnp.dot(normed, w_value, preferred_element_type=jnp.float32).astype(jnp.bfloat16)
    sequences = tokens.shape[0]
    kv_local = cache_keys.shape[1]
    head_dim = cache_keys.shape[2]
    length = cache_keys.shape[3]
    heads_local = stick_bias.shape[0]
    groups = heads_local // kv_local
    query_grid = queries.reshape(sequences, kv_local, groups, head_dim)
    scores = jnp.einsum(
        "skgd,skdc->skgc", query_grid, cache_keys, preferred_element_type=jnp.float32
    ) * head_dim ** (-0.5)
    scores = scores + stick_bias.reshape(kv_local, groups)[None, :, :, None]
    visible = (jnp.arange(length)[None, :] < cache_lengths[:, None])[:, None, None, :]
    log_keep = jnp.where(visible, jax.nn.log_sigmoid(-scores), 0.0)
    later_sum = later_positions(log_keep)
    stick = jnp.where(visible, jnp.exp(jax.nn.log_sigmoid(scores) + later_sum), 0.0).astype(
        jnp.bfloat16
    )
    attended = jnp.einsum(
        "skgc,skdc->skgd", stick, cache_values, preferred_element_type=jnp.float32
    )
    attended = attended.reshape(sequences, heads_local * head_dim).astype(jnp.bfloat16)
    partial_proj = jnp.dot(attended, w_output, preferred_element_type=jnp.float32)
    projected = lax.psum(partial_proj, "tp")
    hidden = layer_norm(normed.astype(jnp.float32) + projected, norm_mid).astype(jnp.bfloat16)
    width = hidden.shape[1]
    topk = routes.shape[1]
    ep_count = lax.axis_size("ep")
    experts = ep_count * expert_gate.shape[0]
    capacity = max(2, (sequences * topk + ep_count - 1) // ep_count)
    flat_routes = routes.reshape(-1)
    onehot = (flat_routes[:, None] == jnp.arange(experts)[None, :]).astype(jnp.float32)
    flat_count = flat_routes.shape[0]
    row_index = jnp.arange(flat_count)
    earlier_table = (row_index[:, None] > row_index[None, :]).astype(jnp.float32)
    before = jnp.dot(earlier_table, onehot, precision=lax.Precision.HIGHEST)
    slot_index = jnp.sum(before * onehot, axis=1).astype(jnp.int32)
    target = flat_routes * capacity + slot_index
    placement = jnp.arange(experts * capacity)[:, None] == target[None, :]
    dispatch = jnp.any(placement.reshape(experts * capacity, sequences, topk), axis=2).astype(
        jnp.bfloat16
    )
    outgoing = jnp.dot(dispatch, hidden, preferred_element_type=jnp.float32).astype(jnp.bfloat16)
    outgoing = outgoing.reshape(ep_count, capacity, width)
    received = lax.all_to_all(outgoing, "ep", split_axis=0, concat_axis=0, tiled=True)
    token_rows = received.reshape(-1, width)
    gate_pre = jnp.dot(token_rows, expert_gate[0], preferred_element_type=jnp.float32)
    up_pre = jnp.dot(token_rows, expert_up[0], preferred_element_type=jnp.float32)
    act = (jax.nn.silu(gate_pre) * up_pre).astype(jnp.bfloat16)
    partial_out = jnp.dot(act, expert_down[0], preferred_element_type=jnp.float32).astype(
        jnp.bfloat16
    )
    expert_out = lax.psum(partial_out, "tp").astype(jnp.float32).astype(jnp.bfloat16)
    returned = lax.all_to_all(
        expert_out.reshape(ep_count, capacity, width), "ep", split_axis=0, concat_axis=0, tiled=True
    )
    selector = jnp.transpose(placement).astype(jnp.bfloat16)
    picked = jnp.dot(selector, returned.reshape(-1, width), preferred_element_type=jnp.float32)
    routed = jnp.sum(picked.reshape(sequences, topk, width) * route_weights[:, :, None], axis=1)
    share = dense_gate.shape[1] // lax.axis_size("tp")
    offset = lax.axis_index("tp") * share
    gate_share = lax.dynamic_slice_in_dim(dense_gate, offset, share, 1)
    up_share = lax.dynamic_slice_in_dim(dense_up, offset, share, 1)
    down_share = lax.dynamic_slice_in_dim(dense_down, offset, share, 0)
    dense_pre = jnp.dot(
        hidden,
        lax.all_gather(gate_share, "ep", axis=0, tiled=True),
        preferred_element_type=jnp.float32,
    )
    dense_lin = jnp.dot(
        hidden,
        lax.all_gather(up_share, "ep", axis=0, tiled=True),
        preferred_element_type=jnp.float32,
    )
    dense_act = (jax.nn.silu(dense_pre) * dense_lin).astype(jnp.bfloat16)
    dense_part = jnp.dot(
        dense_act,
        lax.all_gather(down_share, "ep", axis=1, tiled=True),
        preferred_element_type=jnp.float32,
    )
    dense_out = lax.psum(dense_part.astype(jnp.bfloat16), "tp").astype(jnp.float32)
    mix_weight = jax.nn.sigmoid(
        jnp.dot(hidden.astype(jnp.float32), mix_gate, precision=lax.Precision.HIGHEST)
    )
    combined_rows = hidden.astype(jnp.float32) + routed + mix_weight[:, None] * dense_out
    mixed_rows = layer_norm(combined_rows, norm_out).astype(jnp.bfloat16)
    return (mixed_rows, fresh_keys, fresh_values)


def solution(mesh):
    in_specs = (
        P("ep", None),
        P("ep", "tp", None, None),
        P("ep", "tp", None, None),
        P("ep"),
        P(),
        P(None, "tp"),
        P(None, "tp"),
        P(None, "tp"),
        P("tp"),
        P("tp", None),
        P(),
        P("ep", None),
        P("ep", None),
        P("ep", None, "tp"),
        P("ep", None, "tp"),
        P("ep", "tp", None),
        P("ep", None),
        P("ep", None),
        P(None, "ep"),
        P(),
        P(),
    )
    out_specs = (P("ep", None), P("ep", "tp"), P("ep", "tp"))
    return jax.shard_map(shards, mesh=mesh, in_specs=in_specs, out_specs=out_specs, check_vma=False)
```

profile of v0, /device:TPU:0, one launch (start us, length us, event | category | flops | bytes accessed | tf_op | source)
XLA Modules:
  0.0 213.7 jit_solution(13085332007921850898)
XLA Ops:
  7.2 0.9 iota_compare_fusion.1
  8.1 1.0 convert_reduce_fusion
  9.1 1.0 fusion.36
  10.1 1.6 convolution_convert_fusion.3
  11.7 0.1 reshape.197
  11.8 1.9 fusion.32
  13.7 0.1 reshape.199
  13.8 0.2 reduce_sum.83
  14.0 0.2 fusion.52
  14.2 0.1 copy.43
  14.3 1.0 convolution_add_fusion
  15.3 1.0 reshape.200
  16.3 2.4 %fusion.12 = bf16[16,4,64]{2,1,0:T(4,128)(2,1)S(1)} fusion(bf16[16,1,64,1024]{3,2,1,0:T(8,128)(2,1)} %param.23, f32[16,4,1024]{2,1,0:T(4,128)S(1)} %reshape.200, f32[16,4,1024]{2,1,0:T(4,128)} %get-tuple-element.8, pred[16,1024]{1,0:T(8,128)(4,1)S(1)} %iota_compare_fusion.1), kind=kOutput, calls=%fused_computation.14 | convolution fusion | flops 9113600 | bytes 2646016 | tf_op jit(solution)/shard_map/skgc,skdc->skgd/dot_general | solution.py:74
  18.7 0.1 convert_element_type.81
  18.8 0.9 fusion.70
  19.8 0.8 constant_dynamic-slice_fusion
  20.5 45.3 %all_gather.11 = bf16[128,2048]{1,0:T(8,128)(2,1)S(1)} all-gather(bf16[128,128]{1,0:T(8,128)(2,1)S(1)} %constant_dynamic-slice_fusion), channel_id=1, replica_groups=mesh['ep'=16,'tp'=2] {'ep'}, dimensions={1}, use_global_device_ids=true | all-gather | bytes 557056 | tf_op jit(solution)/shard_map/all_gather | solution.py:133
  65.8 0.8 constant_dynamic-slice_fusion.1
  66.6 38.5 %all_gather.10 = bf16[2048,128]{1,0:T(8,128)(2,1)S(1)} all-gather(bf16[128,128]{1,0:T(8,128)(2,1)S(1)} %constant_dynamic-slice_fusion.1), channel_id=1, replica_groups=mesh['ep'=16,'tp'=2] {'ep'}, dimensions={0}, use_global_device_ids=true | all-gather | bytes 557056 | tf_op jit(solution)/shard_map/all_gather | solution.py:127
  105.1 0.1 copy.44
  105.2 0.1 reshape.202
  105.3 0.2 fusion.16
  105.6 0.1 copy.45
  105.7 0.1 fusion.50
  105.8 1.1 fusion.48
  106.9 1.1 multiply_reduce_fusion.1
  108.1 1.0 multiply_convert_fusion.1
  109.1 1.1 convolution_convert_fusion.1
  110.2 1.9 reshape.203
  112.1 4.2 %all-to-all-start = ((bf16[16,6,2048]{2,1,0:T(8,128)(2,1)}), bf16[16,6,2048]{2,1,0:T(8,128)(2,1)}, u32[]{:S(2)}, u32[]{:S(2)}) async-start(bf16[16,6,2048]{2,1,0:T(8,128)(2,1)} %reshape.203), calls=%async_computation | async-start | bytes 1048576 | tf_op jit(solution)/shard_map/all_to_all | solution.py:100
  116.4 44.2 %all_gather.9 = bf16[2048,128]{1,0:T(8,128)(2,1)S(1)} all-gather(bf16[128,128]{1,0:T(8,128)(2,1)S(1)} %constant_dynamic-slice_fusion.2), channel_id=1, replica_groups=mesh['ep'=16,'tp'=2] {'ep'}, dimensions={0}, use_global_device_ids=true | all-gather | bytes 557056 | tf_op jit(solution)/shard_map/all_gather | solution.py:122
  160.6 0.2 fusion.71
  160.8 1.0 convolution_convert_fusion.2
  161.8 1.2 reshape.204
  163.0 1.5 fusion.24
  164.5 2.3 %convolution_convert_fusion = bf16[96,2048]{1,0:T(8,128)(2,1)S(1)} fusion(bf16[96,2048]{1,0:T(8,128)(2,1)S(1)} %reshape.204, bf16[1,256,2048]{2,1,0:T(8,128)(2,1)} %param.36, bf16[1,2048,256]{2,1,0:T(8,128)(2,1)} %param.35, f32[96,256]{1,0:T(8,128)S(1)} %fusion.24), kind=kOutput, calls=%fused_computation.1 | convolution fusion | flops 201670656 | bytes 2981888 | tf_op jit(solution)/shard_map/dot_general | solution.py:105
  166.8 0.9 reshape.205
  167.8 15.0 %all-reduce.6.cloned.1.call-done = (bf16[16,2048]{1,0:T(8,128)(2,1)}, bf16[16,6,2048]{2,1,0:T(8,128)(2,1)}) async-done(((bf16[16,2048]{1,0:T(8,128)(2,1)}, bf16[16,6,2048]{2,1,0:T(8,128)(2,1)}), (bf16[16,2048]{1,0:T(8,128)(2,1)}, bf16[16,6,2048]{2,1,0:T(8,128)(2,1)})) %all-reduce.6.cloned.1.call-update) | async-done | bytes 458768 | tf_op jit(solution)/shard_map/psum | solution.py:136
  182.8 7.0 %all-to-all-start.1 = ((bf16[16,6,2048]{2,1,0:T(8,128)(2,1)}), bf16[16,6,2048]{2,1,0:T(8,128)(2,1)S(1)}, u32[]{:S(2)}, u32[]{:S(2)}) async-start(bf16[16,6,2048]{2,1,0:T(8,128)(2,1)} %get-tuple-element.4), calls=%async_computation.1 | async-start | bytes 1048576 | tf_op jit(solution)/shard_map/all_to_all | solution.py:109
  189.9 1.8 convolution_convert_fusion.5
  191.7 1.8 convolution_convert_fusion.4
  193.5 0.1 fusion.20
  193.6 11.7 %all-to-all-done.1 = bf16[16,6,2048]{2,1,0:T(8,128)(2,1)S(1)} async-done(((bf16[16,6,2048]{2,1,0:T(8,128)(2,1)}), bf16[16,6,2048]{2,1,0:T(8,128)(2,1)S(1)}, u32[]{:S(2)}, u32[]{:S(2)}) %all-to-all-start.1) | async-done | bytes 393248 | tf_op jit(solution)/shard_map/all_to_all | solution.py:109
  205.3 0.1 reshape.209
  205.4 0.3 fusion.4
  205.7 0.2 fusion.69
  205.9 0.2 multiply_reduce_fusion
  206.1 0.7 multiply_convert_fusion
  (41 shorter events, 0.5 us)
Async XLA Ops:
  7.2 4.6 %copy-start = (bf16[16,1,64,1024]{3,2,1,0:T(8,128)(2,1)S(1)}, bf16[16,1,64,1024]{3,2,1,0:T(8,128)(2,1)}, u32[]{:S(2)}) copy-start(bf16[16,1,64,1024]{3,2,1,0:T(8,128)(2,1)} %param.22) | copy-start | bytes 6291460
  7.2 98.6 %all-reduce.4.cloned.1.call-start = ((), (), s32[]{:S(2)}) async-start(), calls=%async_computation.2 | async-start | bytes 262144 | tf_op jit(solution)/shard_map/psum | solution.py:79
  14.3 4.5 %copy-start.2 = (bf16[256,2048]{1,0:T(8,128)(2,1)S(1)}, bf16[256,2048]{1,0:T(8,128)(2,1)}, u32[]{:S(2)}) copy-start(bf16[256,2048]{1,0:T(8,128)(2,1)} %param.30) | copy-start | bytes 3145732
  16.3 88.8 %copy-start.5 = (s32[16,6]{0,1:T(8,128)S(1)}, s32[16,6]{0,1:T(8,128)}, u32[]{:S(2)}) copy-start(s32[16,6]{0,1:T(8,128)} %param.32) | copy-start | bytes 1156
  18.7 87.0 %copy-start.6 = (bf16[128,256]{1,0:T(8,128)(2,1)S(1)}, bf16[128,256]{1,0:T(8,128)(2,1)}, u32[]{:S(2)}) copy-start(bf16[128,256]{1,0:T(8,128)(2,1)} %param.37) | copy-start | bytes 196612
  18.7 87.1 %copy-start.1 = (bf16[16,2048]{1,0:T(8,128)(2,1)S(1)}, bf16[16,2048]{1,0:T(8,128)(2,1)}, u32[]{:S(2)}) copy-start(bf16[16,2048]{1,0:T(8,128)(2,1)} %param.21) | copy-start | bytes 196612
  18.7 87.1 %copy-start.3 = (f32[2048]{0:T(1024)S(1)}, f32[2048]{0:T(1024)}, u32[]{:S(2)}) copy-start(f32[2048]{0:T(1024)} %param.25) | copy-start | bytes 24580
  18.7 89.3 %copy-start.7 = (f32[2048]{0:T(1024)S(1)}, f32[2048]{0:T(1024)}, u32[]{:S(2)}) copy-start(f32[2048]{0:T(1024)} %param.31) | copy-start | bytes 24580
  112.1 49.7 %all-to-all-start = ((bf16[16,6,2048]{2,1,0:T(8,128)(2,1)}), bf16[16,6,2048]{2,1,0:T(8,128)(2,1)}, u32[]{:S(2)}, u32[]{:S(2)}) async-start(bf16[16,6,2048]{2,1,0:T(8,128)(2,1)} %reshape.203), calls=%async_computation | async-start | bytes 1048576 | tf_op jit(solution)/shard_map/all_to_all | solution.py:100
  116.3 66.5 %all-reduce.6.cloned.1.call-start = ((), (), s32[]{:S(2)}) async-start(), calls=%async_computation.3 | async-start | bytes 1179648 | tf_op jit(solution)/shard_map/psum | solution.py:136
  166.8 26.7 %copy-start.9 = (f32[2048]{0:T(1024)S(1)}, f32[2048]{0:T(1024)}, u32[]{:S(2)}) copy-start(f32[2048]{0:T(1024)} %param.40) | copy-start | bytes 24580
  166.8 38.6 %copy-start.10 = (f32[16,6]{0,1:T(8,128)S(1)}, f32[16,6]{0,1:T(8,128)}, u32[]{:S(2)}) copy-start(f32[16,6]{0,1:T(8,128)} %param.33) | copy-start | bytes 1156
  167.8 38.3 %copy-start.8 = (f32[2048]{0:T(1024)S(1)}, f32[2048]{0:T(1024)}, u32[]{:S(2)}) copy-start(f32[2048]{0:T(1024)} %param.41) | copy-start | bytes 24580
  182.8 22.9 %copy-start.4 = (bf16[16,2048]{1,0:T(8,128)(2,1)S(1)}, bf16[16,2048]{1,0:T(8,128)(2,1)}, u32[]{:S(2)}) copy-start(bf16[16,2048]{1,0:T(8,128)(2,1)} %get-tuple-element.3) | copy-start | bytes 196612
  182.8 22.5 %all-to-all-start.1 = ((bf16[16,6,2048]{2,1,0:T(8,128)(2,1)}), bf16[16,6,2048]{2,1,0:T(8,128)(2,1)S(1)}, u32[]{:S(2)}, u32[]{:S(2)}) async-start(bf16[16,6,2048]{2,1,0:T(8,128)(2,1)} %get-tuple-element.4), calls=%async_computation.1 | async-start | bytes 1048576 | tf_op jit(solution)/shard_map/all_to_all | solution.py:109
Sparse Core Ops, SparseCore 0:
  19.9 20.6 all-reduce.3
  167.9 14.8 all-reduce.5
where the time goes:
time: 215 us; the launch traced here: 214 us
  blocking collectives  128 us (60%)
  waiting for transfers between devices  26.7 us (12%)
  matrix products  18.1 us (8%)
  between operations  14.3 us (7%)
  starting transfers between devices  11.3 us (5%)
  other arithmetic  7.63 us (4%)
  local copies, waits for them, and re-layouts  7.53 us (4%)
    all_gather x1, blocking collectives, shards(): lax.all_gather(down_share, 'ep', axis=1, tiled=True)  45.3 us
    all_gather x1, blocking collectives, shards(): lax.all_gather(gate_share, 'ep', axis=0, tiled=True)  44.2 us
    all_gather x1, blocking collectives, shards(): lax.all_gather(up_share, 'ep', axis=0, tiled=True)  38.5 us
    psum x1, waiting for transfers between devices, shards(): lax.psum(dense_part.astype(jnp.bfloat16), 'tp').astype(jnp.float32)  15 us
    all_to_all x1, waiting for transfers between devices, shards(): lax.all_to_all(expert_out.reshape(ep_count, capacity, width), 'ep', split...  11.7 us
    all_to_all x1, starting transfers between devices, shards(): lax.all_to_all(expert_out.reshape(ep_count, capacity, width), 'ep', split...  6.96 us
  transfers between devices with their start and end apart: 4, of which 2 were waited for; matrix products, arithmetic and copies ran while one was open for 3% of the time, Pallas kernels for 0%

commit v1 on v0

v1 whole, which is shorter than its diff:
```python
import functools

import jax
import jax.numpy as jnp
from jax import lax
from jax.experimental import pallas as pl
from jax.experimental.pallas import tpu as pltpu
from jax.sharding import PartitionSpec as P

MESH = pl.DeviceIdType.MESH
F32 = jnp.float32
BF16 = jnp.bfloat16
LANES = 128


def layer_norm(values, gain):
    center = jnp.mean(values, -1, keepdims=True)
    spread = jnp.mean(jnp.square(values - center), -1, keepdims=True)
    return (values - center) * lax.rsqrt(spread + 1e-05) * gain


def sigmoid(x):
    return 1.0 / (1.0 + jnp.exp(-x))


def iota(shape, dim):
    return lax.broadcasted_iota(jnp.int32, shape, dim)


def bits(n):
    assert n & (n - 1) == 0
    return n.bit_length() - 1


def dot(a, b):
    return jnp.dot(a, b, preferred_element_type=F32)


def dot_nt(a, b):
    return lax.dot_general(a, b, (((1,), (1,)), ((), ())), preferred_element_type=F32)


def dot_tn(a, b):
    return lax.dot_general(a, b, (((0,), (0,)), ((), ())), preferred_element_type=F32)


def layer_kernel(
    ep, slots, chunks, head_dim,
    tokens, norm_in, norm_mid, norm_out, mix_gate, routes, route_weights, lengths, bias,
    wq, wk, wv, keys, values, wo, eg, eu, ed, dg, du, dd,
    mixed, fresh_k, fresh_v,
    wq_v, wk_v, wv_v, k_v, v_v, wo_v, eg_v, eu_v, ed_v, dd_v,
    pack, gath, proj_out, proj_in, outgoing, received, expert_y, returned, fin_out, fin_in,
    load_sem, own_sem, gs, gr, ds, dr, rs, rr, ts, tr,
):
    me = lax.axis_index("ep")
    core = lax.axis_index("tp")
    other = 1 - core
    seqs, width = tokens.shape
    heads = bias.shape[0]
    length = keys.shape[1]
    rows = dg.shape[0]
    share = pack.shape[2]

    barrier = pltpu.get_barrier_semaphore()

    def greet(p, c):
        pl.semaphore_signal(
            barrier, inc=1, device_id=(lax.rem(me + p, ep), core), device_id_type=MESH
        )
        return c

    lax.fori_loop(1, ep, greet, 0)
    pl.semaphore_signal(barrier, inc=1, device_id=(me, other), device_id_type=MESH)

    offset = pl.multiple_of(core * share, share)
    span = keys.shape[0] // chunks
    moves = [
        (dd.at[pl.ds(offset, share), :], dd_v),
        (dg.at[:, pl.ds(offset, share)], pack.at[0]),
        (du.at[:, pl.ds(offset, share)], pack.at[1]),
        (wq, wq_v),
    ]
    moves += [(keys.at[pl.ds(c * span, span)], k_v.at[pl.ds(c * span, span)]) for c in range(chunks)]
    moves += [(values.at[pl.ds(c * span, span)], v_v.at[pl.ds(c * span, span)]) for c in range(chunks)]
    moves += [(wo, wo_v), (wk, wk_v), (wv, wv_v), (eg, eg_v), (eu, eu_v), (ed, ed_v)]
    loads = [pltpu.make_async_copy(a, b, load_sem.at[i]) for i, (a, b) in enumerate(moves)]
    for load in loads:
        load.start()
    key_loads = loads[4 : 4 + chunks]
    value_loads = loads[4 + chunks : 4 + 2 * chunks]
    wo_load, wk_load, wv_load, eg_load, eu_load, ed_load = loads[4 + 2 * chunks :]

    normed = layer_norm(tokens[...].astype(F32), norm_in[...]).astype(BF16)

    for load in loads[:3]:
        load.wait()
    pack[2] = dd_v[...].astype(F32).T.astype(BF16)

    def block(index, size):
        return pl.ds(pl.multiple_of(index * size, size), size)

    pl.semaphore_wait(barrier, ep)

    def gather(p, target):
        return pltpu.make_async_remote_copy(
            src_ref=pack,
            dst_ref=gath.at[:, block(target, rows), :],
            send_sem=gs.at[p],
            recv_sem=gr.at[p],
            device_id=(lax.rem(me + p, ep), core),
            device_id_type=MESH,
        )

    def start_gather(p, c):
        gather(p, me).start()
        return c

    lax.fori_loop(1, ep, start_gather, 0)
    own_gather = pltpu.make_async_copy(pack, gath.at[:, block(me, rows), :], own_sem.at[0])
    own_gather.start()

    total = ep * slots
    slot_of = iota((seqs, total), 1)
    expert_of = lax.shift_right_logical(slot_of, bits(slots))
    place_of = slot_of & (slots - 1)
    route_rows = routes[...]
    weight_rows = route_weights[...]
    member = jnp.zeros((seqs, total), F32)
    weight = jnp.zeros((seqs, total), F32)
    for k in range(route_rows.shape[1]):
        hit = route_rows[:, k : k + 1] == expert_of
        member = jnp.where(hit, 1.0, member)
        weight = jnp.where(hit, weight_rows[:, k : k + 1], weight)
    earlier = jnp.where(iota((seqs, seqs), 0) > iota((seqs, seqs), 1), 1.0, 0.0).astype(BF16)
    before = dot(earlier, member.astype(BF16)).astype(jnp.int32)
    chosen = jnp.where(before == place_of, member, 0.0)
    weight = weight * chosen
    chosen = chosen.astype(BF16)
    w_hi = weight.astype(BF16)
    w_rest = weight - w_hi.astype(F32)
    w_mid = w_rest.astype(BF16)
    w_lo = (w_rest - w_mid.astype(F32)).astype(BF16)
    weight_split = jnp.concatenate([w_hi.astype(F32), w_mid.astype(F32), w_lo.astype(F32)], axis=0).astype(BF16)

    grid_rows = heads * seqs
    flat = heads * head_dim
    col = iota((flat, heads * LANES), 1)
    spread_table = jnp.where(
        iota((flat, heads * LANES), 0)
        == lax.shift_right_logical(col, bits(LANES)) * head_dim + (col & (head_dim - 1)),
        1.0,
        0.0,
    ).astype(BF16)
    own_block = (
        lax.shift_right_logical(iota((grid_rows, seqs * head_dim), 1), bits(head_dim))
        == (iota((grid_rows, seqs * head_dim), 0) & (seqs - 1))
    )
    row = iota((2 * LANES, 2 * LANES), 0) & (LANES - 1)
    column = iota((2 * LANES, 2 * LANES), 1)
    later_table = jnp.where((column >= LANES) | (row > column), 1.0, 0.0).astype(BF16)
    row_seq = iota((grid_rows, 1), 0) & (seqs - 1)
    row_head = lax.shift_right_logical(iota((grid_rows, 1), 0), bits(seqs))
    filled = jnp.zeros((grid_rows, 1), jnp.int32)
    for s in range(seqs):
        filled = jnp.where(row_seq == s, lengths[s], filled)
    row_bias = jnp.zeros((grid_rows, 1), F32)
    for h in range(heads):
        row_bias = jnp.where(row_head == h, bias[h], row_bias)

    loads[3].wait()
    queries = dot(normed, wq_v[...]).astype(BF16)
    twice = dot(queries, spread_table)
    stacked = jnp.concatenate([twice[:, h * LANES : (h + 1) * LANES] for h in range(heads)], axis=0)
    tiled = jnp.concatenate([stacked] * (seqs * head_dim // LANES), axis=1)
    query_grid = jnp.where(own_block, tiled, 0.0).astype(BF16)
    scores = None
    for c in range(chunks):
        key_loads[c].wait()
        part = dot(query_grid[:, c * span : (c + 1) * span], k_v[c * span : (c + 1) * span, :])
        scores = part if scores is None else scores + part
    scores = scores * head_dim ** (-0.5) + row_bias
    visible = iota((grid_rows, length), 1) < filled
    soft = jnp.log1p(jnp.exp(-jnp.abs(scores)))
    log_keep = jnp.where(visible, jnp.minimum(-scores, 0.0) - soft, 0.0)
    log_take = jnp.minimum(scores, 0.0) - soft
    count = length // LANES
    keep_hi = log_keep.astype(BF16).astype(F32)
    keep_lo = log_keep - keep_hi
    stack = jnp.concatenate(
        [
            jnp.concatenate(
                [keep_hi[:, c * LANES : (c + 1) * LANES], keep_lo[:, c * LANES : (c + 1) * LANES]], axis=1
            )
            for c in range(count)
        ],
        axis=0,
    ).astype(BF16)
    sums = dot(stack, later_table)
    carried = jnp.zeros((grid_rows, LANES), F32)
    pieces = [None] * count
    for c in reversed(range(count)):
        here = sums[c * grid_rows : (c + 1) * grid_rows]
        pieces[c] = here[:, :LANES] + carried
        carried = carried + here[:, LANES:]
    later = jnp.concatenate(pieces, axis=1)
    stick = jnp.where(visible, jnp.exp(log_take + later), 0.0).astype(BF16)
    folded = jnp.zeros((grid_rows, LANES), F32)
    for c in range(chunks):
        value_loads[c].wait()
        part = dot_nt(stick, v_v[c * span : (c + 1) * span, :])
        part = jnp.where(own_block[:, c * span : (c + 1) * span], part, 0.0)
        for b in range(span // LANES):
            folded = folded + part[:, b * LANES : (b + 1) * LANES]
    folded = jnp.concatenate([folded[h * seqs : (h + 1) * seqs] for h in range(heads)], axis=1)
    attended = dot_nt(folded.astype(BF16), spread_table).astype(BF16)
    wo_load.wait()
    part_proj = dot(attended, wo_v[...])
    proj_out[...] = part_proj

    def swap(index, source, target):
        return pltpu.make_async_remote_copy(
            src_ref=source,
            dst_ref=target,
            send_sem=ts.at[index],
            recv_sem=tr.at[index],
            device_id=(me, other),
            device_id_type=MESH,
        )

    proj_swap = swap(0, proj_out, proj_in)
    proj_swap.start()
    wk_load.wait()
    fresh_k[...] = dot(normed, wk_v[...]).astype(BF16)
    wv_load.wait()
    fresh_v[...] = dot(normed, wv_v[...]).astype(BF16)
    proj_swap.wait()
    projected = part_proj + proj_in[...]
    hidden = layer_norm(normed.astype(F32) + projected, norm_mid[...]).astype(BF16)

    outgoing[...] = dot_tn(chosen, hidden).astype(BF16)

    def dispatch(p, source, target):
        return pltpu.make_async_remote_copy(
            src_ref=outgoing.at[block(source, slots), :],
            dst_ref=received.at[block(target, slots), :],
            send_sem=ds.at[p],
            recv_sem=dr.at[p],
            device_id=(lax.rem(me + p, ep), core),
            device_id_type=MESH,
        )

    def start_dispatch(p, c):
        dispatch(p, lax.rem(me + p, ep), me).start()
        return c

    lax.fori_loop(1, ep, start_dispatch, 0)
    own_rows = pltpu.make_async_copy(
        outgoing.at[block(me, slots), :], received.at[block(me, slots), :], own_sem.at[1]
    )
    own_rows.start()

    hidden_f = hidden.astype(F32)
    mix_weight = sigmoid(jnp.sum(hidden_f * mix_gate[...], axis=-1, keepdims=True))

    def wait_gather(p, c):
        done = gather(p, lax.rem(me + ep - p, ep))
        done.wait_recv()
        done.wait_send()
        return c

    lax.fori_loop(1, ep, wait_gather, 0)
    own_gather.wait()
    dense_pre = dot(hidden, gath[0])
    dense_lin = dot(hidden, gath[1])
    dense_act = (dense_pre * sigmoid(dense_pre) * dense_lin).astype(BF16)
    dense_part = dot_nt(dense_act, gath[2]) * mix_weight

    eg_load.wait()
    eu_load.wait()
    ed_load.wait()

    def wait_dispatch(p, c):
        source = lax.rem(me + ep - p, ep)
        done = dispatch(p, lax.rem(me + p, ep), source)
        done.wait_recv()
        done.wait_send()
        return c

    lax.fori_loop(1, ep, wait_dispatch, 0)
    own_rows.wait()
    token_rows = received[...]
    gate_pre = dot(token_rows, eg_v[...])
    up_pre = dot(token_rows, eu_v[...])
    act = (gate_pre * sigmoid(gate_pre) * up_pre).astype(BF16)
    expert_y[...] = dot(act, ed_v[...]).astype(BF16)

    def give_back(p, source, target):
        return pltpu.make_async_remote_copy(
            src_ref=expert_y.at[block(source, slots), :],
            dst_ref=returned.at[block(target, slots), :],
            send_sem=rs.at[p],
            recv_sem=rr.at[p],
            device_id=(lax.rem(me + p, ep), core),
            device_id_type=MESH,
        )

    def start_return(p, c):
        give_back(p, lax.rem(me + p, ep), me).start()
        return c

    lax.fori_loop(1, ep, start_return, 0)
    own_back = pltpu.make_async_copy(
        expert_y.at[block(me, slots), :], returned.at[block(me, slots), :], own_sem.at[2]
    )
    own_back.start()

    def wait_return(p, c):
        source = lax.rem(me + ep - p, ep)
        done = give_back(p, lax.rem(me + p, ep), source)
        done.wait_recv()
        done.wait_send()
        return c

    lax.fori_loop(1, ep, wait_return, 0)
    own_back.wait()
    routed3 = dot(weight_split, returned[...])
    routed = routed3[:seqs] + routed3[seqs : 2 * seqs] + routed3[2 * seqs :]
    final = routed + dense_part
    fin_out[...] = final
    fin_swap = swap(1, fin_out, fin_in)
    fin_swap.start()
    fin_swap.wait()
    combined = hidden_f + (final + fin_in[...])
    mixed[...] = layer_norm(combined, norm_out[...]).astype(BF16)


def shards(
    tokens, cache_keys, cache_values, cache_lengths, norm_in, w_query, w_key, w_value, stick_bias,
    w_output, norm_mid, routes, route_weights, expert_gate, expert_up, expert_down,
    dense_gate, dense_up, dense_down, mix_gate, norm_out,
):
    ep = lax.axis_size("ep")
    tp = lax.axis_size("tp")
    seqs, width = tokens.shape
    head_dim, length = cache_keys.shape[2:]
    chunks = 4
    topk = routes.shape[1]
    capacity = max(2, -(-seqs * topk // ep))
    slots = 8
    while slots < capacity:
        slots *= 2
    hidden_units = expert_gate.shape[2]
    rows = dense_gate.shape[0]
    share = dense_gate.shape[1] // tp
    flat_cache = (seqs * head_dim, length)
    total = ep * slots
    vmem = pl.BlockSpec(memory_space=pltpu.VMEM)
    smem = pl.BlockSpec(memory_space=pltpu.SMEM)
    hbm = pl.BlockSpec(memory_space=pl.ANY)
    dma = pltpu.SemaphoreType.DMA
    return pl.pallas_call(
        functools.partial(layer_kernel, ep, slots, chunks, head_dim),
        out_shape=(
            jax.ShapeDtypeStruct((seqs, width), BF16),
            jax.ShapeDtypeStruct((seqs, w_key.shape[1]), BF16),
            jax.ShapeDtypeStruct((seqs, w_value.shape[1]), BF16),
        ),
        in_specs=[vmem] * 7 + [smem] * 2 + [hbm] * 12,
        out_specs=(vmem, vmem, vmem),
        scratch_shapes=[
            pltpu.VMEM(w_query.shape, BF16),
            pltpu.VMEM(w_key.shape, BF16),
            pltpu.VMEM(w_value.shape, BF16),
            pltpu.VMEM(flat_cache, BF16),
            pltpu.VMEM(flat_cache, BF16),
            pltpu.VMEM(w_output.shape, BF16),
            pltpu.VMEM((width, hidden_units), BF16),
            pltpu.VMEM((width, hidden_units), BF16),
            pltpu.VMEM((hidden_units, width), BF16),
            pltpu.VMEM((share, dense_down.shape[1]), BF16),
            pltpu.VMEM((3, rows, share), BF16),
            pltpu.VMEM((3, ep * rows, share), BF16),
            pltpu.VMEM((seqs, width), F32),
            pltpu.VMEM((seqs, width), F32),
            pltpu.VMEM((total, width), BF16),
            pltpu.VMEM((total, width), BF16),
            pltpu.VMEM((total, width), BF16),
            pltpu.VMEM((total, width), BF16),
            pltpu.VMEM((seqs, width), F32),
            pltpu.VMEM((seqs, width), F32),
            dma((10 + 2 * chunks,)),
            dma((3,)),
            dma((ep,)),
            dma((ep,)),
            dma((ep,)),
            dma((ep,)),
            dma((ep,)),
            dma((ep,)),
            dma((2,)),
            dma((2,)),
        ],
        compiler_params=pltpu.CompilerParams(
            collective_id=0, has_side_effects=True, vmem_limit_bytes=60 * 1024 * 1024
        ),
    )(
        tokens,
        norm_in.reshape(1, width),
        norm_mid.reshape(1, width),
        norm_out.reshape(1, width),
        mix_gate.reshape(1, width),
        routes,
        route_weights,
        cache_lengths,
        stick_bias,
        w_query,
        w_key,
        w_value,
        cache_keys.reshape(flat_cache),
        cache_values.reshape(flat_cache),
        w_output,
        expert_gate.reshape(width, hidden_units),
        expert_up.reshape(width, hidden_units),
        expert_down.reshape(hidden_units, width),
        dense_gate,
        dense_up,
        dense_down,
    )


def solution(mesh):
    in_specs = (
        P("ep", None),
        P("ep", "tp", None, None),
        P("ep", "tp", None, None),
        P("ep"),
        P(),
        P(None, "tp"),
        P(None, "tp"),
        P(None, "tp"),
        P("tp"),
        P("tp", None),
        P(),
        P("ep", None),
        P("ep", None),
        P("ep", None, "tp"),
        P("ep", None, "tp"),
        P("ep", "tp", None),
        P("ep", None),
        P("ep", None),
        P(None, "ep"),
        P(),
        P(),
    )
    out_specs = (P("ep", None), P("ep", "tp"), P("ep", "tp"))
    return jax.shard_map(shards, mesh=mesh, in_specs=in_specs, out_specs=out_specs, check_vma=False)
```

time: 215 us -> 82.9 us (0.39)
  the two profiles are of different devices: /device:TPU:0 before, /device:TPU:29 now
where the time goes in v1:
time: 82.9 us; the launch traced here: 82.5 us
  Pallas kernels  71.2 us (86%)
  local copies, waits for them, and re-layouts  10.6 us (13%)
    pallas_call x1, Pallas kernels, shards(): pl.pallas_call(functools.partial(layer_kernel, ep, slots, chunks, head_di...  71.2 us
    unnamed x7, local copies, waits for them, and re-layouts  10.6 us

profile of v1, /device:TPU:29, one launch (start us, length us, event | category | flops | bytes accessed | tf_op | source)
XLA Modules:
  0.0 82.5 jit_solution(11165374984723883737)
XLA Ops:
  0.6 1.4 %copy.24.routes = s32[16,6]{1,0:T(8,128)} copy(s32[16,6]{0,1:T(8,128)} %param.32) | data formatting | bytes 768 | tf_op args[11]
  2.0 1.4 %copy.25.route_weights = f32[16,6]{1,0:T(8,128)} copy(f32[16,6]{0,1:T(8,128)} %param.33) | data formatting | bytes 768 | tf_op args[12]
  3.3 1.9 %copy.26.wk = bf16[2048,64]{1,0:T(8,128)(2,1)} copy(bf16[2048,64]{0,1:T(8,128)(2,1)} %param.27) | data formatting | bytes 524288 | tf_op args[6]
  5.3 2.0 %copy.27.wv = bf16[2048,64]{1,0:T(8,128)(2,1)} copy(bf16[2048,64]{0,1:T(8,128)(2,1)} %param.28) | data formatting | bytes 524288 | tf_op args[7]
  7.3 71.2 %shard_map.220 = (bf16[16,2048]{1,0:T(8,128)(2,1)}, bf16[16,64]{1,0:T(8,128)(2,1)}, bf16[16,64]{1,0:T(8,128)(2,1)}) custom-call(bf16[16,2048]{1,0:T(8,128)(2,1)} %tokens.1, f32[1,2048]{1,0:T(1,128)} %bitcast.14, f32[1,2048]{1,0:T(1,128)} %bitcast.15, f32[1,2048]{1,0:T(1,128)} %bitcast.16, f32[1,2048]{1,0:T(1,128)} %bitcast.17, s32[16,6]{1,0:T(8,128)} %copy.24.routes, ...), custom_call_target="tpu_custom_call" | custom-call | tf_op jit(solution)/shard_map/pallas_call | solution.py:362
  78.5 1.5 %copy.31 = bf16[16,2048]{1,0:T(8,128)(2,1)} copy(bf16[16,2048]{1,0:T(8,128)(2,1)} %get-tuple-element.6) | data formatting | bytes 131072
  80.0 1.3 %copy.32 = bf16[16,64]{1,0:T(8,128)(2,1)} copy(bf16[16,64]{1,0:T(8,128)(2,1)} %get-tuple-element.7) | data formatting | bytes 4096
  81.2 1.3 %copy.33 = bf16[16,64]{1,0:T(8,128)(2,1)} copy(bf16[16,64]{1,0:T(8,128)(2,1)} %get-tuple-element.8) | data formatting | bytes 4096

commit v2 on v1

--- a/solution.py
+++ b/solution.py
@@ -50,8 +50,9 @@
     wq, wk, wv, keys, values, wo, eg, eu, ed, dg, du, dd,
     mixed, fresh_k, fresh_v,
     wq_v, wk_v, wv_v, k_v, v_v, wo_v, eg_v, eu_v, ed_v, dd_v,
-    pack, gath, proj_out, proj_in, outgoing, received, expert_y, returned, fin_out, fin_in,
-    load_sem, own_sem, gs, gr, ds, dr, rs, rr, ts, tr,
+    pack, gath, proj_out, proj_in, hid_v, outgoing, received, received_other, part_out, part_in,
+    expert_y, returned, fin_out, fin_in, mixed_v, fresh_k_v, fresh_v_v,
+    load_sem, own_sem, out_sem, gs, gr, ds, dr, rs, rr, ts, tr,
 ):
     me = lax.axis_index("ep")
     core = lax.axis_index("tp")
@@ -63,6 +64,10 @@
     share = pack.shape[2]
 
     barrier = pltpu.get_barrier_semaphore()
+
+    half = width // 2
+    mine = pl.ds(pl.multiple_of(core * half, half), half)
+    theirs = pl.ds(pl.multiple_of(other * half, half), half)
 
     def greet(p, c):
         pl.semaphore_signal(
@@ -102,46 +107,73 @@
 
     pl.semaphore_wait(barrier, ep)
 
-    def gather(p, target):
+    levels = bits(ep)
+    my_bits = [lax.rem(me // (1 << k), 2) for k in range(levels)]
+
+    def flip(mask):
+        index = me
+        for k in range(levels):
+            if mask >> k & 1:
+                index = index + (1 - 2 * my_bits[k]) * (1 << k)
+        return index
+
+    down = list(reversed(range(levels)))
+    orders = [down, down[:-2] + [0, 1], [0, 1] + down[:-2]]
+    steps = [[] for _ in range(levels)]
+    number = 0
+    for array, order in enumerate(orders):
+        held = [0]
+        for step, bit in enumerate(order):
+            for mask in held:
+                steps[step].append((number, array, mask, mask | 1 << bit, 1 << bit))
+                number += 1
+            held = held + [mask | 1 << bit for mask in held]
+
+    def gather(item, incoming):
+        number, array, mask, far_mask, bit = item
         return pltpu.make_async_remote_copy(
-            src_ref=pack,
-            dst_ref=gath.at[:, block(target, rows), :],
-            send_sem=gs.at[p],
-            recv_sem=gr.at[p],
-            device_id=(lax.rem(me + p, ep), core),
+            src_ref=gath.at[array, block(flip(mask), rows), :] if mask else pack.at[array],
+            dst_ref=gath.at[array, block(flip(far_mask if incoming else mask), rows), :],
+            send_sem=gs.at[number],
+            recv_sem=gr.at[number],
+            device_id=(flip(bit), core),
             device_id_type=MESH,
         )
 
-    def start_gather(p, c):
-        gather(p, me).start()
-        return c
-
-    lax.fori_loop(1, ep, start_gather, 0)
+    def gather_start(step):
+        for item in steps[step]:
+            gather(item, False).start()
+
+    def gather_wait(step):
+        for item in steps[step]:
+            gather(item, True).wait_recv()
+
+    gather_start(0)
     own_gather = pltpu.make_async_copy(pack, gath.at[:, block(me, rows), :], own_sem.at[0])
     own_gather.start()
 
     total = ep * slots
-    slot_of = iota((seqs, total), 1)
+    slot_of = iota((total, seqs), 0)
     expert_of = lax.shift_right_logical(slot_of, bits(slots))
     place_of = slot_of & (slots - 1)
     route_rows = routes[...]
     weight_rows = route_weights[...]
-    member = jnp.zeros((seqs, total), F32)
-    weight = jnp.zeros((seqs, total), F32)
-    for k in range(route_rows.shape[1]):
-        hit = route_rows[:, k : k + 1] == expert_of
+    member = jnp.zeros((total, seqs), F32)
+    weight = jnp.zeros((total, seqs), F32)
+    for k in range(route_rows.shape[0]):
+        hit = route_rows[k : k + 1, :] == expert_of
         member = jnp.where(hit, 1.0, member)
-        weight = jnp.where(hit, weight_rows[:, k : k + 1], weight)
-    earlier = jnp.where(iota((seqs, seqs), 0) > iota((seqs, seqs), 1), 1.0, 0.0).astype(BF16)
-    before = dot(earlier, member.astype(BF16)).astype(jnp.int32)
+        weight = jnp.where(hit, weight_rows[k : k + 1, :], weight)
+    earlier = jnp.where(iota((seqs, seqs), 0) < iota((seqs, seqs), 1), 1.0, 0.0).astype(BF16)
+    before = dot(member.astype(BF16), earlier).astype(jnp.int32)
     chosen = jnp.where(before == place_of, member, 0.0)
-    weight = weight * chosen
+    weight = (weight * chosen).T
     chosen = chosen.astype(BF16)
     w_hi = weight.astype(BF16)
     w_rest = weight - w_hi.astype(F32)
     w_mid = w_rest.astype(BF16)
     w_lo = (w_rest - w_mid.astype(F32)).astype(BF16)
-    weight_split = jnp.concatenate([w_hi.astype(F32), w_mid.astype(F32), w_lo.astype(F32)], axis=0).astype(BF16)
+    weight_split = jnp.concatenate([w_hi, w_mid, w_lo], axis=0)
 
     grid_rows = heads * seqs
     flat = heads * head_dim
@@ -179,6 +211,8 @@
         key_loads[c].wait()
         part = dot(query_grid[:, c * span : (c + 1) * span], k_v[c * span : (c + 1) * span, :])
         scores = part if scores is None else scores + part
+    gather_wait(0)
+    gather_start(1)
     scores = scores * head_dim ** (-0.5) + row_bias
     visible = iota((grid_rows, length), 1) < filled
     soft = jnp.log1p(jnp.exp(-jnp.abs(scores)))
@@ -205,6 +239,9 @@
         carried = carried + here[:, LANES:]
     later = jnp.concatenate(pieces, axis=1)
     stick = jnp.where(visible, jnp.exp(log_take + later), 0.0).astype(BF16)
+    if levels > 2:
+        gather_wait(1)
+        gather_start(2)
     folded = jnp.zeros((grid_rows, LANES), F32)
     for c in range(chunks):
         value_loads[c].wait()
@@ -230,15 +267,25 @@
 
     proj_swap = swap(0, proj_out, proj_in)
     proj_swap.start()
+    for step in range(3, levels):
+        gather_wait(step - 1)
+        gather_start(step)
     wk_load.wait()
-    fresh_k[...] = dot(normed, wk_v[...]).astype(BF16)
+    fresh_k_v[...] = dot_nt(normed, wk_v[...]).astype(BF16)
     wv_load.wait()
-    fresh_v[...] = dot(normed, wv_v[...]).astype(BF16)
+    fresh_v_v[...] = dot_nt(normed, wv_v[...]).astype(BF16)
+    fresh_out = [
+        pltpu.make_async_copy(fresh_k_v, fresh_k, out_sem.at[0]),
+        pltpu.make_async_copy(fresh_v_v, fresh_v, out_sem.at[1]),
+    ]
+    for copy in fresh_out:
+        copy.start()
     proj_swap.wait()
     projected = part_proj + proj_in[...]
     hidden = layer_norm(normed.astype(F32) + projected, norm_mid[...]).astype(BF16)
 
-    outgoing[...] = dot_tn(chosen, hidden).astype(BF16)
+    hid_v[...] = hidden
+    outgoing[...] = dot(chosen, hid_v[:, mine]).astype(BF16)
 
     def dispatch(p, source, target):
         return pltpu.make_async_remote_copy(
@@ -263,13 +310,10 @@
     hidden_f = hidden.astype(F32)
     mix_weight = sigmoid(jnp.sum(hidden_f * mix_gate[...], axis=-1, keepdims=True))
 
-    def wait_gather(p, c):
-        done = gather(p, lax.rem(me + ep - p, ep))
-        done.wait_recv()
-        done.wait_send()
-        return c
-
-    lax.fori_loop(1, ep, wait_gather, 0)
+    gather_wait(levels - 1)
+    for step in range(levels):
+        for item in steps[step]:
+            gather(item, False).wait_send()
     own_gather.wait()
     dense_pre = dot(hidden, gath[0])
     dense_lin = dot(hidden, gath[1])
@@ -289,11 +333,22 @@
 
     lax.fori_loop(1, ep, wait_dispatch, 0)
     own_rows.wait()
-    token_rows = received[...]
-    gate_pre = dot(token_rows, eg_v[...])
-    up_pre = dot(token_rows, eu_v[...])
+    row_swap = swap(2, received, received_other)
+    row_swap.start()
+    near = received[...]
+    gate_pre = dot(near, eg_v[mine, :])
+    up_pre = dot(near, eu_v[mine, :])
+    row_swap.wait()
+    far = received_other[...]
+    gate_pre = gate_pre + dot(far, eg_v[theirs, :])
+    up_pre = up_pre + dot(far, eu_v[theirs, :])
     act = (gate_pre * sigmoid(gate_pre) * up_pre).astype(BF16)
-    expert_y[...] = dot(act, ed_v[...]).astype(BF16)
+    part_out[...] = dot(act, ed_v[:, theirs]).astype(BF16)
+    part_swap = swap(3, part_out, part_in)
+    part_swap.start()
+    own_part = dot(act, ed_v[:, mine]).astype(BF16).astype(F32)
+    part_swap.wait()
+    expert_y[...] = (own_part + part_in[...].astype(F32)).astype(BF16)
 
     def give_back(p, source, target):
         return pltpu.make_async_remote_copy(
@@ -326,13 +381,18 @@
     own_back.wait()
     routed3 = dot(weight_split, returned[...])
     routed = routed3[:seqs] + routed3[seqs : 2 * seqs] + routed3[2 * seqs :]
-    final = routed + dense_part
-    fin_out[...] = final
+    fin_out[...] = dense_part
+    fin_out[:, mine] = fin_out[:, mine] + routed
     fin_swap = swap(1, fin_out, fin_in)
     fin_swap.start()
+    for copy in fresh_out:
+        copy.wait()
     fin_swap.wait()
-    combined = hidden_f + (final + fin_in[...])
-    mixed[...] = layer_norm(combined, norm_out[...]).astype(BF16)
+    combined = hidden_f + (fin_out[...] + fin_in[...])
+    mixed_v[...] = layer_norm(combined, norm_out[...]).astype(BF16)
+    result = pltpu.make_async_copy(mixed_v, mixed, out_sem.at[2])
+    result.start()
+    result.wait()
 
 
 def shards(
@@ -358,6 +418,8 @@
     vmem = pl.BlockSpec(memory_space=pltpu.VMEM)
     smem = pl.BlockSpec(memory_space=pltpu.SMEM)
     hbm = pl.BlockSpec(memory_space=pl.ANY)
+    hbm_out = pl.BlockSpec(memory_space=pltpu.HBM)
+    half = width // 2
     dma = pltpu.SemaphoreType.DMA
     return pl.pallas_call(
         functools.partial(layer_kernel, ep, slots, chunks, head_dim),
@@ -367,11 +429,11 @@
             jax.ShapeDtypeStruct((seqs, w_value.shape[1]), BF16),
         ),
         in_specs=[vmem] * 7 + [smem] * 2 + [hbm] * 12,
-        out_specs=(vmem, vmem, vmem),
+        out_specs=(hbm_out, hbm_out, hbm_out),
         scratch_shapes=[
             pltpu.VMEM(w_query.shape, BF16),
-            pltpu.VMEM(w_key.shape, BF16),
-            pltpu.VMEM(w_value.shape, BF16),
+            pltpu.VMEM(w_key.shape[::-1], BF16),
+            pltpu.VMEM(w_value.shape[::-1], BF16),
             pltpu.VMEM(flat_cache, BF16),
             pltpu.VMEM(flat_cache, BF16),
             pltpu.VMEM(w_output.shape, BF16),
@@ -383,22 +445,24 @@
             pltpu.VMEM((3, ep * rows, share), BF16),
             pltpu.VMEM((seqs, width), F32),
             pltpu.VMEM((seqs, width), F32),
-            pltpu.VMEM((total, width), BF16),
-            pltpu.VMEM((total, width), BF16),
-            pltpu.VMEM((total, width), BF16),
-            pltpu.VMEM((total, width), BF16),
+            pltpu.VMEM((seqs, width), BF16),
+            *[pltpu.VMEM((total, half), BF16)] * 7,
             pltpu.VMEM((seqs, width), F32),
             pltpu.VMEM((seqs, width), F32),
+            pltpu.VMEM((seqs, width), BF16),
+            pltpu.VMEM((seqs, w_key.shape[1]), BF16),
+            pltpu.VMEM((seqs, w_value.shape[1]), BF16),
             dma((10 + 2 * chunks,)),
             dma((3,)),
+            dma((3,)),
+            dma((3 * ep,)),
+            dma((3 * ep,)),
             dma((ep,)),
             dma((ep,)),
             dma((ep,)),
             dma((ep,)),
-            dma((ep,)),
-            dma((ep,)),
-            dma((2,)),
-            dma((2,)),
+            dma((4,)),
+            dma((4,)),
         ],
         compiler_params=pltpu.CompilerParams(
             collective_id=0, has_side_effects=True, vmem_limit_bytes=60 * 1024 * 1024
@@ -409,13 +473,13 @@
         norm_mid.reshape(1, width),
         norm_out.reshape(1, width),
         mix_gate.reshape(1, width),
-        routes,
-        route_weights,
+        routes.T,
+        route_weights.T,
         cache_lengths,
         stick_bias,
         w_query,
-        w_key,
-        w_value,
+        w_key.T,
+        w_value.T,
         cache_keys.reshape(flat_cache),
         cache_values.reshape(flat_cache),
         w_output,

time: 82.9 us -> 53.1 us (0.64)
  the two profiles are of different devices: /device:TPU:29 before, /device:TPU:0 now
where the time goes in v2:
time: 53.1 us; the launch traced here: 52.3 us
  Pallas kernels  47.6 us (90%)
  local copies, waits for them, and re-layouts  4.02 us (8%)
  between operations  0.65 us (1%)
    pallas_call x1, Pallas kernels, shards(): pl.pallas_call(functools.partial(layer_kernel, ep, slots, chunks, head_di...  47.6 us
    unnamed x3, local copies, waits for them, and re-layouts  4.02 us

profile of v2, /device:TPU:0, one launch (start us, length us, event | category | flops | bytes accessed | tf_op | source)
XLA Modules:
  0.0 52.3 jit_solution(6222171112025471463)
XLA Ops:
  0.6 47.6 %shard_map.220 = (bf16[16,2048]{1,0:T(8,128)(2,1)}, bf16[16,64]{1,0:T(8,128)(2,1)}, bf16[16,64]{1,0:T(8,128)(2,1)}) custom-call(bf16[16,2048]{1,0:T(8,128)(2,1)} %tokens.1, f32[1,2048]{1,0:T(1,128)} %bitcast.20, f32[1,2048]{1,0:T(1,128)} %bitcast.21, f32[1,2048]{1,0:T(1,128)} %bitcast.22, f32[1,2048]{1,0:T(1,128)} %bitcast.23, s32[6,16]{1,0:T(8,128)} %bitcast.24, ...), custom_call_target="tpu_custom_call" | custom-call | tf_op jit(solution)/shard_map/pallas_call | solution.py:424
  48.2 1.5 %copy.27 = bf16[16,2048]{1,0:T(8,128)(2,1)} copy(bf16[16,2048]{1,0:T(8,128)(2,1)} %get-tuple-element.6) | data formatting | bytes 131072
  49.7 1.3 %copy.28 = bf16[16,64]{1,0:T(8,128)(2,1)} copy(bf16[16,64]{1,0:T(8,128)(2,1)} %get-tuple-element.7) | data formatting | bytes 4096
  51.0 1.3 %copy.29 = bf16[16,64]{1,0:T(8,128)(2,1)} copy(bf16[16,64]{1,0:T(8,128)(2,1)} %get-tuple-element.8) | data formatting | bytes 4096

commit v3 on v2

--- a/solution.py
+++ b/solution.py
@@ -11,6 +11,7 @@
 F32 = jnp.float32
 BF16 = jnp.bfloat16
 LANES = 128
+PLAN = (3, 4, 5)
 
 
 def layer_norm(values, gain):
@@ -46,13 +47,13 @@
 
 def layer_kernel(
     ep, slots, chunks, head_dim,
-    tokens, norm_in, norm_mid, norm_out, mix_gate, routes, route_weights, lengths, bias,
+    tokens, norm_in, norm_mid, mix_gate, routes, route_weights, lengths, bias,
     wq, wk, wv, keys, values, wo, eg, eu, ed, dg, du, dd,
-    mixed, fresh_k, fresh_v,
+    combined, fresh_k, fresh_v,
     wq_v, wk_v, wv_v, k_v, v_v, wo_v, eg_v, eu_v, ed_v, dd_v,
     pack, gath, proj_out, proj_in, hid_v, outgoing, received, received_other, part_out, part_in,
-    expert_y, returned, fin_out, fin_in, mixed_v, fresh_k_v, fresh_v_v,
-    load_sem, own_sem, out_sem, gs, gr, ds, dr, rs, rr, ts, tr,
+    expert_y, returned, fin_out, fin_in,
+    load_sem, own_sem, gs, gr, ds, dr, rs, rr, ts, tr,
 ):
     me = lax.axis_index("ep")
     core = lax.axis_index("tp")
@@ -97,60 +98,6 @@
     wo_load, wk_load, wv_load, eg_load, eu_load, ed_load = loads[4 + 2 * chunks :]
 
     normed = layer_norm(tokens[...].astype(F32), norm_in[...]).astype(BF16)
-
-    for load in loads[:3]:
-        load.wait()
-    pack[2] = dd_v[...].astype(F32).T.astype(BF16)
-
-    def block(index, size):
-        return pl.ds(pl.multiple_of(index * size, size), size)
-
-    pl.semaphore_wait(barrier, ep)
-
-    levels = bits(ep)
-    my_bits = [lax.rem(me // (1 << k), 2) for k in range(levels)]
-
-    def flip(mask):
-        index = me
-        for k in range(levels):
-            if mask >> k & 1:
-                index = index + (1 - 2 * my_bits[k]) * (1 << k)
-        return index
-
-    down = list(reversed(range(levels)))
-    orders = [down, down[:-2] + [0, 1], [0, 1] + down[:-2]]
-    steps = [[] for _ in range(levels)]
-    number = 0
-    for array, order in enumerate(orders):
-        held = [0]
-        for step, bit in enumerate(order):
-            for mask in held:
-                steps[step].append((number, array, mask, mask | 1 << bit, 1 << bit))
-                number += 1
-            held = held + [mask | 1 << bit for mask in held]
-
-    def gather(item, incoming):
-        number, array, mask, far_mask, bit = item
-        return pltpu.make_async_remote_copy(
-            src_ref=gath.at[array, block(flip(mask), rows), :] if mask else pack.at[array],
-            dst_ref=gath.at[array, block(flip(far_mask if incoming else mask), rows), :],
-            send_sem=gs.at[number],
-            recv_sem=gr.at[number],
-            device_id=(flip(bit), core),
-            device_id_type=MESH,
-        )
-
-    def gather_start(step):
-        for item in steps[step]:
-            gather(item, False).start()
-
-    def gather_wait(step):
-        for item in steps[step]:
-            gather(item, True).wait_recv()
-
-    gather_start(0)
-    own_gather = pltpu.make_async_copy(pack, gath.at[:, block(me, rows), :], own_sem.at[0])
-    own_gather.start()
 
     total = ep * slots
     slot_of = iota((total, seqs), 0)
@@ -200,6 +147,66 @@
     for h in range(heads):
         row_bias = jnp.where(row_head == h, bias[h], row_bias)
 
+    for load in loads[:3]:
+        load.wait()
+    pack[2] = dd_v[...].astype(F32).T.astype(BF16)
+
+    def block(index, size):
+        return pl.ds(pl.multiple_of(index * size, size), size)
+
+    pl.semaphore_wait(barrier, ep)
+
+    levels = bits(ep)
+    my_bits = [lax.rem(me // (1 << k), 2) for k in range(levels)]
+
+    def flip(mask):
+        index = me
+        for k in range(levels):
+            if mask >> k & 1:
+                index = index + (1 - 2 * my_bits[k]) * (1 << k)
+        return index
+
+    down = list(reversed(range(levels)))
+    orders = [down, down[:-2] + [0, 1], [0, 1] + down[:-2]]
+    steps = [[] for _ in range(levels)]
+    number = 0
+    for array, order in enumerate(orders):
+        held = [0]
+        for step, bit in enumerate(order):
+            for mask in held:
+                steps[step].append((number, array, mask, mask | 1 << bit, 1 << bit))
+                number += 1
+            held = held + [mask | 1 << bit for mask in held]
+
+    def gather(item, incoming):
+        number, array, mask, far_mask, bit = item
+        return pltpu.make_async_remote_copy(
+            src_ref=gath.at[array, block(flip(mask), rows), :] if mask else pack.at[array],
+            dst_ref=gath.at[array, block(flip(far_mask if incoming else mask), rows), :],
+            send_sem=gs.at[number],
+            recv_sem=gr.at[number],
+            device_id=(flip(bit), core),
+            device_id_type=MESH,
+        )
+
+    def gather_start(step):
+        for item in steps[step]:
+            gather(item, False).start()
+
+    def gather_wait(step):
+        for item in steps[step]:
+            gather(item, True).wait_recv()
+
+    def advance(point):
+        for step in range(1, levels):
+            if PLAN[min(step - 1, len(PLAN) - 1)] == point:
+                gather_wait(step - 1)
+                gather_start(step)
+
+    gather_start(0)
+    own_gather = pltpu.make_async_copy(pack, gath.at[:, block(me, rows), :], own_sem.at[0])
+    own_gather.start()
+
     loads[3].wait()
     queries = dot(normed, wq_v[...]).astype(BF16)
     twice = dot(queries, spread_table)
@@ -211,8 +218,7 @@
         key_loads[c].wait()
         part = dot(query_grid[:, c * span : (c + 1) * span], k_v[c * span : (c + 1) * span, :])
         scores = part if scores is None else scores + part
-    gather_wait(0)
-    gather_start(1)
+    advance(1)
     scores = scores * head_dim ** (-0.5) + row_bias
     visible = iota((grid_rows, length), 1) < filled
     soft = jnp.log1p(jnp.exp(-jnp.abs(scores)))
@@ -239,9 +245,7 @@
         carried = carried + here[:, LANES:]
     later = jnp.concatenate(pieces, axis=1)
     stick = jnp.where(visible, jnp.exp(log_take + later), 0.0).astype(BF16)
-    if levels > 2:
-        gather_wait(1)
-        gather_start(2)
+    advance(2)
     folded = jnp.zeros((grid_rows, LANES), F32)
     for c in range(chunks):
         value_loads[c].wait()
@@ -267,19 +271,11 @@
 
     proj_swap = swap(0, proj_out, proj_in)
     proj_swap.start()
-    for step in range(3, levels):
-        gather_wait(step - 1)
-        gather_start(step)
+    advance(3)
     wk_load.wait()
-    fresh_k_v[...] = dot_nt(normed, wk_v[...]).astype(BF16)
+    fresh_k[...] = dot_nt(normed, wk_v[...]).astype(BF16)
     wv_load.wait()
-    fresh_v_v[...] = dot_nt(normed, wv_v[...]).astype(BF16)
-    fresh_out = [
-        pltpu.make_async_copy(fresh_k_v, fresh_k, out_sem.at[0]),
-        pltpu.make_async_copy(fresh_v_v, fresh_v, out_sem.at[1]),
-    ]
-    for copy in fresh_out:
-        copy.start()
+    fresh_v[...] = dot_nt(normed, wv_v[...]).astype(BF16)
     proj_swap.wait()
     projected = part_proj + proj_in[...]
     hidden = layer_norm(normed.astype(F32) + projected, norm_mid[...]).astype(BF16)
@@ -310,15 +306,7 @@
     hidden_f = hidden.astype(F32)
     mix_weight = sigmoid(jnp.sum(hidden_f * mix_gate[...], axis=-1, keepdims=True))
 
-    gather_wait(levels - 1)
-    for step in range(levels):
-        for item in steps[step]:
-            gather(item, False).wait_send()
-    own_gather.wait()
-    dense_pre = dot(hidden, gath[0])
-    dense_lin = dot(hidden, gath[1])
-    dense_act = (dense_pre * sigmoid(dense_pre) * dense_lin).astype(BF16)
-    dense_part = dot_nt(dense_act, gath[2]) * mix_weight
+    advance(4)
 
     eg_load.wait()
     eu_load.wait()
@@ -335,6 +323,7 @@
     own_rows.wait()
     row_swap = swap(2, received, received_other)
     row_swap.start()
+    advance(5)
     near = received[...]
     gate_pre = dot(near, eg_v[mine, :])
     up_pre = dot(near, eu_v[mine, :])
@@ -346,6 +335,7 @@
     part_out[...] = dot(act, ed_v[:, theirs]).astype(BF16)
     part_swap = swap(3, part_out, part_in)
     part_swap.start()
+    advance(6)
     own_part = dot(act, ed_v[:, mine]).astype(BF16).astype(F32)
     part_swap.wait()
     expert_y[...] = (own_part + part_in[...].astype(F32)).astype(BF16)
@@ -369,6 +359,17 @@
         expert_y.at[block(me, slots), :], returned.at[block(me, slots), :], own_sem.at[2]
     )
     own_back.start()
+    advance(7)
+    gather_wait(levels - 1)
+    for step in range(levels):
+        for item in steps[step]:
+            gather(item, False).wait_send()
+    own_gather.wait()
+    dense_pre = dot(hidden, gath[0])
+    dense_lin = dot(hidden, gath[1])
+    dense_act = (dense_pre * sigmoid(dense_pre) * dense_lin).astype(BF16)
+    dense_part = dot_nt(dense_act, gath[2]) * mix_weight
+
 
     def wait_return(p, c):
         source = lax.rem(me + ep - p, ep)
@@ -385,14 +386,14 @@
     fin_out[:, mine] = fin_out[:, mine] + routed
     fin_swap = swap(1, fin_out, fin_in)
     fin_swap.start()
-    for copy in fresh_out:
-        copy.wait()
     fin_swap.wait()
-    combined = hidden_f + (fin_out[...] + fin_in[...])
-    mixed_v[...] = layer_norm(combined, norm_out[...]).astype(BF16)
-    result = pltpu.make_async_copy(mixed_v, mixed, out_sem.at[2])
-    result.start()
-    result.wait()
+    combined[...] = hidden_f + (fin_out[...] + fin_in[...])
+
+
+def finish_kernel(combined, norm_out, fresh_k, fresh_v, mixed, out_k, out_v):
+    mixed[...] = layer_norm(combined[...], norm_out[...]).astype(BF16)
+    out_k[...] = fresh_k[...]
+    out_v[...] = fresh_v[...]
 
 
 def shards(
@@ -418,18 +419,17 @@
     vmem = pl.BlockSpec(memory_space=pltpu.VMEM)
     smem = pl.BlockSpec(memory_space=pltpu.SMEM)
     hbm = pl.BlockSpec(memory_space=pl.ANY)
-    hbm_out = pl.BlockSpec(memory_space=pltpu.HBM)
     half = width // 2
     dma = pltpu.SemaphoreType.DMA
-    return pl.pallas_call(
+    combined, fresh_k, fresh_v = pl.pallas_call(
         functools.partial(layer_kernel, ep, slots, chunks, head_dim),
         out_shape=(
-            jax.ShapeDtypeStruct((seqs, width), BF16),
+            jax.ShapeDtypeStruct((seqs, width), F32),
             jax.ShapeDtypeStruct((seqs, w_key.shape[1]), BF16),
             jax.ShapeDtypeStruct((seqs, w_value.shape[1]), BF16),
         ),
-        in_specs=[vmem] * 7 + [smem] * 2 + [hbm] * 12,
-        out_specs=(hbm_out, hbm_out, hbm_out),
+        in_specs=[vmem] * 6 + [smem] * 2 + [hbm] * 12,
+        out_specs=(vmem, vmem, vmem),
         scratch_shapes=[
             pltpu.VMEM(w_query.shape, BF16),
             pltpu.VMEM(w_key.shape[::-1], BF16),
@@ -449,11 +449,7 @@
             *[pltpu.VMEM((total, half), BF16)] * 7,
             pltpu.VMEM((seqs, width), F32),
             pltpu.VMEM((seqs, width), F32),
-            pltpu.VMEM((seqs, width), BF16),
-            pltpu.VMEM((seqs, w_key.shape[1]), BF16),
-            pltpu.VMEM((seqs, w_value.shape[1]), BF16),
             dma((10 + 2 * chunks,)),
-            dma((3,)),
             dma((3,)),
             dma((3 * ep,)),
             dma((3 * ep,)),
@@ -471,7 +467,6 @@
         tokens,
         norm_in.reshape(1, width),
         norm_mid.reshape(1, width),
-        norm_out.reshape(1, width),
         mix_gate.reshape(1, width),
         routes.T,
         route_weights.T,
@@ -490,6 +485,14 @@
         dense_up,
         dense_down,
     )
+    return pl.pallas_call(
+        finish_kernel,
+        out_shape=(
+            jax.ShapeDtypeStruct((seqs, width), BF16),
+            jax.ShapeDtypeStruct(fresh_k.shape, BF16),
+            jax.ShapeDtypeStruct(fresh_v.shape, BF16),
+        ),
+    )(combined, norm_out.reshape(1, width), fresh_k, fresh_v)
 
 
 def solution(mesh):

time: 53.1 us -> 42.7 us (0.80); the launches traced: 52.3 us -> 42.5 us
  Pallas kernels: 47.6 us -> 41.9 us
  local copies, waits for them, and re-layouts: 4.02 us -> 0 us
    pallas_call x1, Pallas kernels: 47.6 us -> 40.1 us  [shards(): pl.pallas_call(functools.partial(layer_kernel, ep, slots, chunks, head_di...]
    unnamed x3 -> x0, local copies, waits for them, and re-layouts: 4.02 us -> none
    pallas_call x0 -> x1, Pallas kernels: none -> 1.77 us  [shards(): pl.pallas_call(finish_kernel, out_shape=(jax.ShapeDtypeStruct((seqs, widt...]
where the time goes in v3:
time: 42.7 us; the launch traced here: 42.5 us
  Pallas kernels  41.9 us (98%)
  between operations  0.65 us (2%)
    pallas_call x1, Pallas kernels, shards(): pl.pallas_call(functools.partial(layer_kernel, ep, slots, chunks, head_di...  40.1 us
    pallas_call x1, Pallas kernels, shards(): pl.pallas_call(finish_kernel, out_shape=(jax.ShapeDtypeStruct((seqs, widt...  1.77 us

profile of v3, /device:TPU:0, one launch (start us, length us, event | category | flops | bytes accessed | tf_op | source)
XLA Modules:
  0.0 42.5 jit_solution(10630104937442664124)
XLA Ops:
  0.6 40.1 %shard_map.220 = (f32[16,2048]{1,0:T(8,128)}, bf16[16,64]{1,0:T(8,128)(2,1)}, bf16[16,64]{1,0:T(8,128)(2,1)}) custom-call(bf16[16,2048]{1,0:T(8,128)(2,1)} %tokens.1, f32[1,2048]{1,0:T(1,128)} %bitcast.21, f32[1,2048]{1,0:T(1,128)} %bitcast.22, f32[1,2048]{1,0:T(1,128)} %bitcast.23, s32[6,16]{1,0:T(8,128)} %bitcast.24, f32[6,16]{1,0:T(8,128)} %bitcast.25, ...), custom_call_target="tpu_custom_call" | custom-call | tf_op jit(solution)/shard_map/pallas_call | solution.py:424
  40.8 1.8 %shard_map.221 = (bf16[16,2048]{1,0:T(8,128)(2,1)}, bf16[16,64]{1,0:T(8,128)(2,1)}, bf16[16,64]{1,0:T(8,128)(2,1)}) custom-call(f32[16,2048]{1,0:T(8,128)} %get-tuple-element.6.combined, f32[1,2048]{1,0:T(1,128)} %bitcast.20, bf16[16,64]{1,0:T(8,128)(2,1)} %get-tuple-element.7.fresh_k, bf16[16,64]{1,0:T(8,128)(2,1)} %get-tuple-element.8.fresh_v), custom_call_target="tpu_custom_call" | custom-call | tf_op jit(solution)/shard_map/pallas_call | solution.py:488

commit v4 on v3

--- a/solution.py
+++ b/solution.py
@@ -11,7 +11,7 @@
 F32 = jnp.float32
 BF16 = jnp.bfloat16
 LANES = 128
-PLAN = (3, 4, 5)
+PLAN = ((3, 4, 5), (3, 4, 5), (2, 3, 4))
 
 
 def layer_norm(values, gain):
@@ -199,9 +199,14 @@
 
     def advance(point):
         for step in range(1, levels):
-            if PLAN[min(step - 1, len(PLAN) - 1)] == point:
-                gather_wait(step - 1)
-                gather_start(step)
+            for array, plan in enumerate(PLAN):
+                if plan[min(step - 1, len(plan) - 1)] == point:
+                    for item in steps[step - 1]:
+                        if item[1] == array:
+                            gather(item, True).wait_recv()
+                    for item in steps[step]:
+                        if item[1] == array:
+                            gather(item, False).start()
 
     gather_start(0)
     own_gather = pltpu.make_async_copy(pack, gath.at[:, block(me, rows), :], own_sem.at[0])

time: 42.7 us -> 41.1 us (0.963)
  Pallas kernels: 41.9 us -> 40.2 us
    pallas_call x1, Pallas kernels: 40.1 us -> 38.5 us  [shards(): pl.pallas_call(functools.partial(layer_kernel, ep, slots, chunks, head_di...]
where the time goes in v4:
time: 41.1 us; the launch traced here: 40.9 us
  Pallas kernels  40.2 us (98%)
  between operations  0.65 us (2%)
    pallas_call x1, Pallas kernels, shards(): pl.pallas_call(functools.partial(layer_kernel, ep, slots, chunks, head_di...  38.5 us
    pallas_call x1, Pallas kernels, shards(): pl.pallas_call(finish_kernel, out_shape=(jax.ShapeDtypeStruct((seqs, widt...  1.77 us

profile of v4, /device:TPU:0, one launch (start us, length us, event | category | flops | bytes accessed | tf_op | source)
XLA Modules:
  0.0 40.9 jit_solution(8053365842729847421)
XLA Ops:
  0.6 38.5 %shard_map.220 = (f32[16,2048]{1,0:T(8,128)}, bf16[16,64]{1,0:T(8,128)(2,1)}, bf16[16,64]{1,0:T(8,128)(2,1)}) custom-call(bf16[16,2048]{1,0:T(8,128)(2,1)} %tokens.1, f32[1,2048]{1,0:T(1,128)} %bitcast.21, f32[1,2048]{1,0:T(1,128)} %bitcast.22, f32[1,2048]{1,0:T(1,128)} %bitcast.23, s32[6,16]{1,0:T(8,128)} %bitcast.24, f32[6,16]{1,0:T(8,128)} %bitcast.25, ...), custom_call_target="tpu_custom_call" | custom-call | tf_op jit(solution)/shard_map/pallas_call | solution.py:429
  39.1 1.8 %shard_map.221 = (bf16[16,2048]{1,0:T(8,128)(2,1)}, bf16[16,64]{1,0:T(8,128)(2,1)}, bf16[16,64]{1,0:T(8,128)(2,1)}) custom-call(f32[16,2048]{1,0:T(8,128)} %get-tuple-element.6.combined, f32[1,2048]{1,0:T(1,128)} %bitcast.20, bf16[16,64]{1,0:T(8,128)(2,1)} %get-tuple-element.7.fresh_k, bf16[16,64]{1,0:T(8,128)(2,1)} %get-tuple-element.8.fresh_v), custom_call_target="tpu_custom_call" | custom-call | tf_op jit(solution)/shard_map/pallas_call | solution.py:493
